TPU v7x, 32 devices: a whole 2x2x4 slice. The times are simulated.
32 devices in a mesh: sp: 4 (over z), tp: 8 (over y, x, core).
Axes of the slice: x: 2, y: 2, z: 4, core: 2. Of those that a mesh axis runs over, the one named last changes fastest.
Arguments:
- target_rows: bfloat16 [768, 2048], P(('sp', 'tp')), may hold values from -6 to 6
- source_rows: bfloat16 [4096, 2048], P(('sp', 'tp')), may hold values from -6 to 6
- target_gain: float32 [2048], replicated, may hold values from 0.55 to 9
- source_gain: float32 [2048], replicated, may hold values from 0.55 to 9
- query_weight: bfloat16 [2048, 2048], P(None, 'tp'), may hold values from -0.125 to 0.125
- key_weight: bfloat16 [2048, 512], P('tp'), may hold values from -0.125 to 0.125
- value_weight: bfloat16 [2048, 512], P('tp'), may hold values from -0.125 to 0.125
- out_weight: bfloat16 [2048, 2048], P('tp'), may hold values from -0.125 to 0.125
- out_cotangent: bfloat16 [768, 2048], P(('sp', 'tp')), may hold values from -6 to 6
Outputs:
- target_grad: float32 [768, 2048], P(('sp', 'tp'))
- source_grad: float32 [4096, 2048], P(('sp', 'tp'))
- out_weight_grad: float32 [2048, 2048], P('tp')
All inputs are finite; a program needn't handle non-finite values.
Results may differ from a plain program's by a relative error of at most 0.03.
Values may be sent and summed in bfloat16 or wider, within the bound.
A program may use at most 64 MiB of HBM per device.

v0:
```python
import jax
import jax.numpy as jnp
from jax import lax
from jax.sharding import PartitionSpec as P

HEAD_DIM = 64
KV_HEADS = 8
EPSILON = 1e-06
NEGATIVE = -1e30


def normalize(matrix, gain_vector):
    widened = matrix.astype(jnp.float32)
    factor = lax.rsqrt(jnp.mean(widened * widened, axis=-1, keepdims=True) + EPSILON)
    return (widened * factor * gain_vector).astype(jnp.bfloat16)


def norm_back(matrix, gain_vector, upstream):
    widened = matrix.astype(jnp.float32)
    factor = lax.rsqrt(jnp.mean(widened * widened, axis=-1, keepdims=True) + EPSILON)
    weighted = upstream * gain_vector
    inner_sum = jnp.mean(weighted * widened, axis=-1, keepdims=True)
    return factor * weighted - widened * factor**3 * inner_sum


def block_rows_for(length):
    return 512 if length % 512 == 0 else length


def body(
    target_rows,
    source_rows,
    target_gain,
    source_gain,
    query_weight,
    key_weight,
    value_weight,
    out_weight,
    out_cotangent,
):
    tp_count = lax.axis_size("tp")
    local_heads = query_weight.shape[1] // HEAD_DIM
    slot_heads = max(1, KV_HEADS // tp_count)
    copies = max(1, tp_count // KV_HEADS)
    per_slot = local_heads // slot_heads
    score_scale = HEAD_DIM ** (-0.5)
    normed_t = normalize(target_rows, target_gain)
    normed_s = normalize(source_rows, source_gain)
    source_local = normed_s.shape[0]
    key_full, value_full = (
        lax.all_gather(key_weight, "tp", axis=0, tiled=True),
        lax.all_gather(value_weight, "tp", axis=0, tiled=True),
    )
    key_own = jnp.dot(normed_s, key_full, preferred_element_type=jnp.float32).astype(jnp.bfloat16)
    value_own = jnp.dot(normed_s, value_full, preferred_element_type=jnp.float32).astype(
        jnp.bfloat16
    )

    def to_slots(matrix):
        split_heads = matrix.reshape(source_local, KV_HEADS, 1, HEAD_DIM)
        spread = jnp.broadcast_to(split_heads, (source_local, KV_HEADS, copies, HEAD_DIM))
        return spread.reshape(source_local, tp_count, slot_heads * HEAD_DIM)

    key_slots, value_slots = (
        lax.all_to_all(to_slots(key_own), "tp", split_axis=1, concat_axis=0, tiled=True),
        lax.all_to_all(to_slots(value_own), "tp", split_axis=1, concat_axis=0, tiled=True),
    )
    source_block = key_slots.shape[0]
    key_flat = key_slots.reshape(source_block, slot_heads * HEAD_DIM)
    value_flat = value_slots.reshape(source_block, slot_heads * HEAD_DIM)
    pieces = lax.all_gather((normed_t, out_cotangent), "tp", axis=0, tiled=True)
    queries = jnp.dot(pieces[0], query_weight, preferred_element_type=jnp.float32).astype(
        jnp.bfloat16
    )
    d_attended = jnp.dot(pieces[1], out_weight.T, preferred_element_type=jnp.float32).astype(
        jnp.bfloat16
    )
    queries, d_attended, cotangent_block = (queries, d_attended, pieces[1])
    target_block = queries.shape[0]
    query_view = queries.reshape(target_block, slot_heads, per_slot, HEAD_DIM)
    start_state = (
        jnp.full((slot_heads, per_slot, target_block), NEGATIVE, jnp.float32),
        jnp.zeros((slot_heads, per_slot, target_block), jnp.float32),
        jnp.zeros((slot_heads, per_slot, target_block, HEAD_DIM), jnp.float32),
    )
    running = start_state
    pieces = (
        lax.all_gather(key_flat, "sp", axis=0, tiled=True),
        lax.all_gather(value_flat, "sp", axis=0, tiled=True),
    )
    length = pieces[0].shape[0]
    step_rows = 2048

    def one_block(carried, block_index):
        prior_max, prior_total, prior_sum = carried
        key_part = lax.dynamic_slice_in_dim(pieces[0], block_index * step_rows, step_rows, 0)
        value_part = lax.dynamic_slice_in_dim(pieces[1], block_index * step_rows, step_rows, 0)
        key_part = key_part.reshape(step_rows, slot_heads, HEAD_DIM)
        value_part = value_part.reshape(step_rows, slot_heads, HEAD_DIM)
        scores = (
            jnp.einsum("tgqd,sgd->gqts", query_view, key_part, preferred_element_type=jnp.float32)
            * score_scale
        )
        new_max = jnp.maximum(prior_max, jnp.max(scores, axis=-1))
        rescale = jnp.exp(prior_max - new_max)
        weights = jnp.exp(scores - new_max[..., None])
        new_total = prior_total * rescale + jnp.sum(weights, axis=-1)
        new_sum = prior_sum * rescale[..., None] + jnp.einsum(
            "gqts,sgd->gqtd",
            weights.astype(jnp.bfloat16),
            value_part,
            preferred_element_type=jnp.float32,
        )
        return ((new_max, new_total, new_sum), None)

    running, unused = lax.scan(one_block, running, jnp.arange(length // step_rows))
    row_max, total, summed = running
    attended = (
        (summed / total[..., None])
        .transpose(2, 0, 1, 3)
        .reshape(target_block, local_heads * HEAD_DIM)
        .astype(jnp.bfloat16)
    )
    log_total = (row_max + jnp.log(total)).transpose(2, 0, 1).reshape(target_block, local_heads)
    delta = jnp.sum(
        (d_attended.astype(jnp.float32) * attended.astype(jnp.float32)).reshape(
            target_block, local_heads, HEAD_DIM
        ),
        axis=-1,
    )
    all_queries, all_grads = (
        lax.all_gather(queries, "sp", axis=0, tiled=True),
        lax.all_gather(d_attended, "sp", axis=0, tiled=True),
    )
    all_logs, all_deltas = (
        lax.all_gather(log_total, "sp", axis=0, tiled=True),
        lax.all_gather(delta, "sp", axis=0, tiled=True),
    )
    whole_rows = all_queries.shape[0]
    step_rows = block_rows_for(whole_rows)
    block_shape = (whole_rows // step_rows, step_rows, slot_heads, per_slot)
    query_blocks = all_queries.reshape(block_shape + (HEAD_DIM,))
    grad_blocks = all_grads.reshape(block_shape + (HEAD_DIM,))
    log_blocks = all_logs.reshape(block_shape)
    delta_blocks = all_deltas.reshape(block_shape)

    def backward_block(sums_so_far, inputs):
        key_sum, value_sum = sums_so_far
        query_part, grad_part, log_part, delta_part = inputs
        scores = (
            jnp.einsum("tgqd,sgd->gqts", query_part, key_slots, preferred_element_type=jnp.float32)
            * score_scale
        )
        probs = jnp.exp(scores - log_part.transpose(1, 2, 0)[..., None])
        value_sum = value_sum + jnp.einsum(
            "gqts,tgqd->sgd",
            probs.astype(jnp.bfloat16),
            grad_part,
            preferred_element_type=jnp.float32,
        )
        d_probs = jnp.einsum(
            "tgqd,sgd->gqts", grad_part, value_slots, preferred_element_type=jnp.float32
        )
        d_scores = (probs * (d_probs - delta_part.transpose(1, 2, 0)[..., None])).astype(
            jnp.bfloat16
        )
        d_query = (
            jnp.einsum("gqts,sgd->tgqd", d_scores, key_slots, preferred_element_type=jnp.float32)
            * score_scale
        )
        key_sum = (
            key_sum
            + jnp.einsum("gqts,tgqd->sgd", d_scores, query_part, preferred_element_type=jnp.float32)
            * score_scale
        )
        return ((key_sum, value_sum), d_query)

    zero_sums = jnp.zeros((source_block, slot_heads, HEAD_DIM), jnp.float32)
    (key_sum, value_sum), d_query = lax.scan(
        backward_block,
        (zero_sums, zero_sums),
        (query_blocks, grad_blocks, log_blocks, delta_blocks),
    )
    query_terms = d_query.reshape(whole_rows, local_heads * HEAD_DIM)
    query_grad = lax.psum_scatter(query_terms, "sp", scatter_dimension=0, tiled=True).astype(
        jnp.bfloat16
    )
    key_back, value_back = (
        lax.all_to_all(key_sum, "tp", split_axis=0, concat_axis=1, tiled=True),
        lax.all_to_all(value_sum, "tp", split_axis=0, concat_axis=1, tiled=True),
    )

    def from_slots(matrix):
        folded = jnp.sum(matrix.reshape(source_local, KV_HEADS, copies, HEAD_DIM), axis=2)
        return folded.reshape(source_local, KV_HEADS * HEAD_DIM).astype(jnp.bfloat16)

    key_grad = from_slots(key_back)
    value_grad = from_slots(value_back)
    d_normed_s = jnp.dot(key_grad, key_full.T, preferred_element_type=jnp.float32) + jnp.dot(
        value_grad, value_full.T, preferred_element_type=jnp.float32
    )
    source_grad = norm_back(source_rows, source_gain, d_normed_s)
    d_normed_t = lax.psum_scatter(
        jnp.dot(query_grad, query_weight.T, preferred_element_type=jnp.float32),
        "tp",
        scatter_dimension=0,
        tiled=True,
    )
    target_grad = out_cotangent.astype(jnp.float32) + norm_back(
        target_rows, target_gain, d_normed_t
    )
    weight_part = jnp.dot(attended.T, cotangent_block, preferred_element_type=jnp.float32)
    out_weight_grad = lax.psum(weight_part, "sp")
    return (target_grad, source_grad, out_weight_grad)


def solution(mesh):
    return jax.shard_map(
        body,
        mesh=mesh,
        in_specs=(
            P(("sp", "tp"), None),
            P(("sp", "tp"), None),
            P(),
            P(),
            P(None, "tp"),
            P("tp", None),
            P("tp", None),
            P("tp", None),
            P(("sp", "tp"), None),
        ),
        out_specs=(P(("sp", "tp"), None), P(("sp", "tp"), None), P("tp", None)),
        check_vma=False,
    )
```

profile of v0, /device:TPU:0, one launch (start us, length us, event | category | flops | bytes accessed | tf_op | source)
XLA Modules:
  0.0 356.4 jit_solution(7738776949373914293)
XLA Ops:
  11.3 11.9 %all_gather.31 = bf16[192,2048]{1,0:T(8,128)(2,1)S(1)} all-gather(bf16[24,2048]{1,0:T(8,128)(2,1)S(1)} %fusion.44), channel_id=1, replica_groups=mesh['sp'=4,'tp'=8] {'tp'}, dimensions={0}, use_global_device_ids=true | all-gather | bytes 884736 | tf_op jit(solution)/shard_map/all_gather | solution.py:71
  24.3 15.0 %all_gather.32 = bf16[768,256]{1,0:T(8,128)(2,1)S(1)} all-gather(bf16[192,256]{1,0:T(8,128)(2,1)S(1)} %convolution_convert_fusion.3), channel_id=1, replica_groups=mesh['sp'=4,'tp'=8] {'sp'}, dimensions={0}, use_global_device_ids=true | all-gather | bytes 491520 | tf_op jit(solution)/shard_map/all_gather | solution.py:132
  40.7 11.7 %all_gather.37 = bf16[192,2048]{1,0:T(8,128)(2,1)S(1)} all-gather(bf16[24,2048]{1,0:T(8,128)(2,1)} %param.19), channel_id=1, replica_groups=mesh['sp'=4,'tp'=8] {'tp'}, dimensions={0}, use_global_device_ids=true | all-gather | bytes 884736 | tf_op jit(solution)/shard_map/all_gather | solution.py:71
  55.8 3.4 all-to-all-start
  59.2 11.9 %all-gather.7.cloned.1.call-done = bf16[2048,512]{1,0:T(8,128)(2,1)} async-done(((bf16[256,512]{1,0:T(8,128)(2,1)}), bf16[2048,512]{1,0:T(8,128)(2,1)}) %all-gather.7.cloned.1.call-update) | async-done | bytes 2097168 | tf_op jit(solution)/shard_map/all_gather | solution.py:52
  74.0 3.4 all-to-all-start.1
  78.3 16.4 %all_gather.33 = bf16[4096,64]{0,1:T(8,128)(2,1)S(1)} all-gather(bf16[1024,64]{0,1:T(8,128)(2,1)S(1)} %bitcast.239), channel_id=1, replica_groups=mesh['sp'=4,'tp'=8] {'sp'}, dimensions={0}, use_global_device_ids=true | all-gather | bytes 655360 | tf_op jit(solution)/shard_map/all_gather | solution.py:88
  95.6 16.0 %all_gather.35 = bf16[4096,64]{0,1:T(8,128)(2,1)S(1)} all-gather(bf16[1024,64]{0,1:T(8,128)(2,1)S(1)} %bitcast.240), channel_id=1, replica_groups=mesh['sp'=4,'tp'=8] {'sp'}, dimensions={0}, use_global_device_ids=true | all-gather | bytes 655360 | tf_op jit(solution)/shard_map/all_gather | solution.py:89
  111.6 23.4 %while.3 = (s32[]{:T(128)}, f32[1,4,192]{2,1,0:T(4,128)S(1)}, f32[1,4,192]{2,1,0:T(4,128)S(1)}, f32[1,4,192,64]{2,3,1,0:T(8,128)S(1)}, s32[2]{0:T(128)S(1)}, /*i...) while((s32[]{:T(128)}, f32[1,4,192]{2,1,0:T(4,128)S(1)}, ...), condition=%wide.region_5.6_spmd.clone, body=%wide.region_2.5_spmd.clone.sunk | while | flops 415388160 | bytes 45173076 | solution.py:116
  112.9 4.6 %bitcast_reduce_fusion.3 = (f32[4,192]{1,0:T(4,128)S(1)}, f32[2048,192,4]{0,1,2:T(8,128)}) fusion(bf16[192,1,4,64]{0,3,2,1:T(8,128)(2,1)} %get-tuple-element.230, bf16[4096,64]{0,1:T(8,128)(2,1)S(1)} %get-tuple-element.229, s32[]{:T(128)S(6)} %select_n.6), kind=kOutput, calls=%fused_computation.1.clone.1 | convolution fusion | flops 204471552 | bytes 6654980 | tf_op jit(solution)/shard_map/while/body/eval_jaxpr/tgqd,sgd->gqts/dot_general | solution.py:101
  117.5 4.3 %fusion.90 = f32[1,4,192,64]{2,3,1,0:T(8,128)S(1)} fusion(f32[2048,192,4]{0,1,2:T(8,128)} %get-tuple-element.198, f32[4,192]{1,0:T(4,128)S(1)} %bitcast.230, f32[1,4,192,64]{2,3,1,0:T(8,128)S(1)} %get-tuple-element.215, bf16[4096,64]{0,1:T(8,128)(2,1)S(1)} %get-tuple-element.231, s32[]{:T(128)S(6)} %select_n.6, f32[4,192]{1,0:T(4,128)S(1)} %get-tuple-element.199, ...), kind=kOutput, calls=%fused_computation.8.clone.1 | convolution fusion | flops 206192640 | bytes 7020549 | tf_op jit(solution)/shard_map/while/body/eval_jaxpr/gqts,sgd->gqtd/dot_general | solution.py:108
  124.6 4.6 %bitcast_reduce_fusion.3 = (f32[4,192]{1,0:T(4,128)S(1)}, f32[2048,192,4]{0,1,2:T(8,128)}) fusion(bf16[192,1,4,64]{0,3,2,1:T(8,128)(2,1)} %get-tuple-element.230, bf16[4096,64]{0,1:T(8,128)(2,1)S(1)} %get-tuple-element.229, s32[]{:T(128)S(6)} %select_n.6), kind=kOutput, calls=%fused_computation.1.clone.1 | convolution fusion | flops 204471552 | bytes 6654980 | tf_op jit(solution)/shard_map/while/body/eval_jaxpr/tgqd,sgd->gqts/dot_general | solution.py:101
  129.2 4.3 %fusion.90 = f32[1,4,192,64]{2,3,1,0:T(8,128)S(1)} fusion(f32[2048,192,4]{0,1,2:T(8,128)} %get-tuple-element.198, f32[4,192]{1,0:T(4,128)S(1)} %bitcast.230, f32[1,4,192,64]{2,3,1,0:T(8,128)S(1)} %get-tuple-element.215, bf16[4096,64]{0,1:T(8,128)(2,1)S(1)} %get-tuple-element.231, s32[]{:T(128)S(6)} %select_n.6, f32[4,192]{1,0:T(4,128)S(1)} %get-tuple-element.199, ...), kind=kOutput, calls=%fused_computation.8.clone.1 | convolution fusion | flops 206192640 | bytes 7020549 | tf_op jit(solution)/shard_map/while/body/eval_jaxpr/gqts,sgd->gqtd/dot_general | solution.py:108
  136.9 15.1 %all_gather.38 = bf16[768,256]{1,0:T(8,128)(2,1)S(1)} all-gather(bf16[192,256]{1,0:T(8,128)(2,1)S(1)} %get-tuple-element.140), channel_id=1, replica_groups=mesh['sp'=4,'tp'=8] {'sp'}, dimensions={0}, use_global_device_ids=true | all-gather | bytes 491520 | tf_op jit(solution)/shard_map/all_gather | solution.py:133
  152.3 13.2 %all-gather.1 = f32[4,192,4]{1,2,0:T(4,128)S(1)} all-gather(f32[1,192,4]{1,2,0:T(4,128)S(1)} %bitcast.250), channel_id=1, replica_groups=mesh['sp'=4,'tp'=8] {'sp'}, dimensions={0}, use_global_device_ids=true | all-gather | bytes 15360 | tf_op jit(solution)/shard_map/all_gather | solution.py:137
  165.8 14.5 %all-gather = f32[768,1,4]{2,1,0:T(1,128)S(1)} all-gather(f32[192,1,4]{2,1,0:T(1,128)S(1)} %bitcast.247), channel_id=2, replica_groups=mesh['sp'=4,'tp'=8] {'sp'}, dimensions={0}, use_global_device_ids=true | all-gather | bytes 15360 | tf_op jit(solution)/shard_map/all_gather | solution.py:136
  183.3 3.2 fusion.27
  191.6 23.7 %reduce-scatter.7.cloned.1.call-done = f32[192,256]{1,0:T(8,128)} async-done(((f32[768,256]{1,0:T(8,128)}), f32[192,256]{1,0:T(8,128)}) %reduce-scatter.7.cloned.1.call-update) | async-done | bytes 196624
  218.0 4.8 %fusion.35 = bf16[1024,1,64]{0,2,1:T(8,128)(2,1)S(1)} fusion(bf16[768,4,64]{0,2,1:T(8,128)(2,1)S(1)} %bitcast.225, bf16[4,768,1024]{1,2,0:T(8,128)(2,1)} %copy-done.3), kind=kOutput, calls=%fused_computation.43 | convolution fusion | flops 402784256 | bytes 6815744 | tf_op jit(solution)/shard_map/while/body/eval_jaxpr/gqts,tgqd->sgd/dot_general | solution.py:173
  225.1 3.6 %all-to-all-start.2 = ((bf16[8,2,4096]{2,1,0:T(2,128)(2,1)}), bf16[8,2,4096]{2,1,0:T(2,128)(2,1)S(1)}, u32[]{:S(2)}, u32[]{:S(2)}) async-start(bf16[8,2,4096]{2,1,0:T(2,128)(2,1)} %reshape.187), calls=%async_computation.3 | async-start | bytes 262144 | tf_op jit(solution)/shard_map/all_to_all | solution.py:189
  228.7 6.9 %fusion.31 = bf16[1024,1,64]{0,2,1:T(8,128)(2,1)S(1)} fusion(bf16[768,4,64]{0,2,1:T(8,128)(2,1)S(1)} %bitcast.228, f32[1024,768,4]{1,0,2:T(8,128)} %copy-done.2, f32[4,768]{1,0:T(4,128)S(1)} %copy.81), kind=kOutput, calls=%fused_computation.40 | convolution fusion | flops 412090368 | bytes 13119488 | tf_op jit(solution)/shard_map/while/body/eval_jaxpr/gqts,tgqd->sgd/dot_general | solution.py:155
  237.4 4.2 %all-to-all-start.3 = ((bf16[8,2,4096]{2,1,0:T(2,128)(2,1)}), bf16[8,2,4096]{2,1,0:T(2,128)(2,1)S(1)}, u32[]{:S(2)}, u32[]{:S(2)}) async-start(bf16[8,2,4096]{2,1,0:T(2,128)(2,1)} %reshape.189), calls=%async_computation.4 | async-start | bytes 262144 | tf_op jit(solution)/shard_map/all_to_all | solution.py:190
  254.1 3.6 %reduce-scatter.5.cloned.1.call-done = f32[24,2048]{1,0:T(8,128)} async-done(((f32[192,2048]{1,0:T(8,128)}), f32[24,2048]{1,0:T(8,128)}) %reduce-scatter.5.cloned.1.call-update) | async-done | bytes 196624 | tf_op jit(solution)/shard_map/reduce_scatter | solution.py:203
  260.5 86.2 %all-reduce.2.cloned.1.call-done = f32[256,2048]{1,0:T(8,128)} async-done(((f32[256,2048]{1,0:T(8,128)}), f32[256,2048]{1,0:T(8,128)}) %all-reduce.2.cloned.1.call-update) | async-done | bytes 2097168 | tf_op jit(solution)/shard_map/psum | solution.py:213
  (131 shorter events, 54.3 us)
Async XLA Ops:
  7.2 16.0 %copy-start = (bf16[2048,256]{1,0:T(8,128)(2,1)S(1)}, bf16[2048,256]{1,0:T(8,128)(2,1)}, u32[]{:S(2)}) copy-start(bf16[2048,256]{1,0:T(8,128)(2,1)} %param.15) | copy-start | bytes 3145732
  7.2 45.8 %copy-start.4 = (bf16[128,2048]{1,0:T(8,128)(2,1)S(1)}, bf16[128,2048]{1,0:T(8,128)(2,1)}, u32[]{:S(2)}) copy-start(bf16[128,2048]{1,0:T(8,128)(2,1)} %param.12) | copy-start | bytes 1572868
  7.2 45.8 %copy-start.11 = (f32[2048]{0:T(1024)S(1)}, f32[2048]{0:T(1024)}, u32[]{:S(2)}) copy-start(f32[2048]{0:T(1024)} %param.14) | copy-start | bytes 24580
  7.2 45.8 %all-gather.5.cloned.1.call-start = ((), (), s32[]{:S(2)}) async-start(), calls=%async_computation.6 | async-start | bytes 2359296 | tf_op jit(solution)/shard_map/all_gather | solution.py:51
  7.9 63.2 %all-gather.7.cloned.1.call-start = ((), (), s32[]{:S(2)}) async-start(), calls=%async_computation.7 | async-start | bytes 2359296 | tf_op jit(solution)/shard_map/all_gather | solution.py:52
  53.0 42.6 %copy-start.15 = (f32[128]{0:T(128)}, f32[128]{0:T(128)S(1)}, u32[]{:S(2)}) copy-start(f32[128]{0:T(128)S(1)} %get-tuple-element.136) | copy-start | bytes 1540
  55.8 18.2 %all-to-all-start = ((bf16[128,8,64]{0,2,1:T(8,128)(2,1)}), bf16[128,8,64]{0,2,1:T(8,128)(2,1)S(1)}, u32[]{:S(2)}, u32[]{:S(2)}) async-start(bf16[128,8,64]{0,2,1:T(8,128)(2,1)} %bitcast), calls=%async_computation | async-start | bytes 262144 | tf_op jit(solution)/shard_map/all_to_all | solution.py:65
  74.0 20.7 %all-to-all-start.1 = ((bf16[128,8,64]{0,2,1:T(8,128)(2,1)}), bf16[128,8,64]{0,2,1:T(8,128)(2,1)S(1)}, u32[]{:S(2)}, u32[]{:S(2)}) async-start(bf16[128,8,64]{0,2,1:T(8,128)(2,1)} %bitcast.7), calls=%async_computation.1 | async-start | bytes 262144 | tf_op jit(solution)/shard_map/all_to_all | solution.py:66
  77.4 137.9 %reduce-scatter.7.cloned.1.call-start = ((), (), s32[]{:S(2)}) async-start(), calls=%async_computation.10 | async-start | bytes 983040
  117.5 5.8 %copy-start.18 = (s32[2]{0:T(128)S(1)}, s32[2]{0:T(128)}, u32[]{:S(2)}) copy-start(s32[2]{0:T(128)} %copy-done.17) | copy-start | bytes 28 | tf_op jit(solution)/shard_map/while
  129.2 4.6 %copy-start.1 = (f32[2048,192,4]{0,1,2:T(8,128)S(1)}, f32[2048,192,4]{0,1,2:T(8,128)}, u32[]{:S(2)}) copy-start(f32[2048,192,4]{0,1,2:T(8,128)} %get-tuple-element.198) | copy-start | bytes 18874372 | tf_op jit(solution)/shard_map/while
  129.2 5.8 %copy-start.18 = (s32[2]{0:T(128)S(1)}, s32[2]{0:T(128)}, u32[]{:S(2)}) copy-start(s32[2]{0:T(128)} %copy-done.17) | copy-start | bytes 28 | tf_op jit(solution)/shard_map/while
  191.5 66.2 %reduce-scatter.5.cloned.1.call-start = ((), (), s32[]{:S(2)}) async-start(), calls=%async_computation.8 | async-start | bytes 1769472 | tf_op jit(solution)/shard_map/reduce_scatter | solution.py:203
  225.1 12.3 %all-to-all-start.2 = ((bf16[8,2,4096]{2,1,0:T(2,128)(2,1)}), bf16[8,2,4096]{2,1,0:T(2,128)(2,1)S(1)}, u32[]{:S(2)}, u32[]{:S(2)}) async-start(bf16[8,2,4096]{2,1,0:T(2,128)(2,1)} %reshape.187), calls=%async_computation.3 | async-start | bytes 262144 | tf_op jit(solution)/shard_map/all_to_all | solution.py:189
  236.5 13.7 %copy-start.5 = (bf16[128,2048]{1,0:T(8,128)(2,1)S(1)}, bf16[128,2048]{1,0:T(8,128)(2,1)}, u32[]{:S(2)}) copy-start(bf16[128,2048]{1,0:T(8,128)(2,1)} %param.12) | copy-start | bytes 1572868
  236.5 13.7 %copy-start.12 = (f32[2048]{0:T(1024)S(1)}, f32[2048]{0:T(1024)}, u32[]{:S(2)}) copy-start(f32[2048]{0:T(1024)} %param.14) | copy-start | bytes 24580
  237.4 9.7 %all-to-all-start.3 = ((bf16[8,2,4096]{2,1,0:T(2,128)(2,1)}), bf16[8,2,4096]{2,1,0:T(2,128)(2,1)S(1)}, u32[]{:S(2)}, u32[]{:S(2)}) async-start(bf16[8,2,4096]{2,1,0:T(2,128)(2,1)} %reshape.189), calls=%async_computation.4 | async-start | bytes 262144 | tf_op jit(solution)/shard_map/all_to_all | solution.py:190
  241.6 105.1 %all-reduce.2.cloned.1.call-start = ((), (), s32[]{:S(2)}) async-start(), calls=%async_computation.9 | async-start | bytes 4194304 | tf_op jit(solution)/shard_map/psum | solution.py:213
  243.4 9.4 %copy-start.14 = (f32[128]{0:T(128)S(1)}, f32[128]{0:T(128)}, u32[]{:S(2)}) copy-start(f32[128]{0:T(128)} %get-tuple-element.135) | copy-start | bytes 1540
  243.4 9.4 %copy-start.16 = (f32[128]{0:T(128)S(1)}, f32[128]{0:T(128)}, u32[]{:S(2)}) copy-start(f32[128]{0:T(128)} %copy-done.15) | copy-start | bytes 1540
  244.1 13.6 %copy-start.6 = (bf16[24,2048]{1,0:T(8,128)(2,1)S(1)}, bf16[24,2048]{1,0:T(8,128)(2,1)}, u32[]{:S(2)}) copy-start(bf16[24,2048]{1,0:T(8,128)(2,1)} %param.11) | copy-start | bytes 294916
  244.1 13.6 %copy-start.10 = (f32[2048]{0:T(1024)S(1)}, f32[2048]{0:T(1024)}, u32[]{:S(2)}) copy-start(f32[2048]{0:T(1024)} %param.13) | copy-start | bytes 24580
  247.4 11.4 %copy-start.9 = (bf16[24,2048]{1,0:T(8,128)(2,1)S(1)}, bf16[24,2048]{1,0:T(8,128)(2,1)}, u32[]{:S(2)}) copy-start(bf16[24,2048]{1,0:T(8,128)(2,1)} %param.19) | copy-start | bytes 294916
  247.4 11.4 %copy-start.13 = (f32[24]{0:T(128)S(1)}, f32[24]{0:T(128)}, u32[]{:S(2)}) copy-start(f32[24]{0:T(128)} %get-tuple-element.137) | copy-start | bytes 292
  (7 other events, 21.6 us)
Sparse Core Ops, SparseCore 0:
  9.9 30.4 all-gather.4
  42.3 28.7 all-gather.6
  191.7 23.5 reduce-scatter.6
  218.4 39.2 reduce-scatter.4
  260.5 86.1 all-reduce.1
where the time goes:
time: 358 us; the launch traced here: 356 us
  waiting for transfers between devices  130 us (36%)
  blocking collectives  114 us (32%)
  matrix products  51.2 us (14%)
  local copies, waits for them, and re-layouts  18.9 us (5%)
  starting transfers between devices  14.7 us (4%)
  between operations  14.2 us (4%)
  other arithmetic  12.3 us (3%)
    psum x1, waiting for transfers between devices, body(): out_weight_grad = lax.psum(weight_part, 'sp')  86.2 us
    unnamed x6, waiting for transfers between devices  25.1 us
    all_gather x2, blocking collectives, body(): pieces = lax.all_gather((normed_t, out_cotangent), 'tp', axis=0, tiled=True)  23.6 us
    all_gather x1, blocking collectives, body(): lax.all_gather(key_flat, 'sp', axis=0, tiled=True)  16.4 us
    all_gather x1, blocking collectives, body(): lax.all_gather(value_flat, 'sp', axis=0, tiled=True)  16 us
    all_gather x1, blocking collectives, body(): lax.all_gather(d_attended, 'sp', axis=0, tiled=True)  15.1 us
    all_gather x1, blocking collectives, body(): lax.all_gather(queries, 'sp', axis=0, tiled=True)  15 us
    all_gather x1, blocking collectives, body(): lax.all_gather(log_total, 'sp', axis=0, tiled=True)  14.5 us
  transfers between devices with their start and end apart: 9, of which 5 were waited for; matrix products, arithmetic and copies ran while one was open for 11% of the time, Pallas kernels for 0%

commit v1 on v0

--- a/solution.py
+++ b/solution.py
@@ -210,7 +210,11 @@
         target_rows, target_gain, d_normed_t
     )
     weight_part = jnp.dot(attended.T, cotangent_block, preferred_element_type=jnp.float32)
-    out_weight_grad = lax.psum(weight_part, "sp")
+    out_weight_grad = weight_part
+    for hop in (1, 2):
+        out_weight_grad = out_weight_grad + lax.ppermute(
+            out_weight_grad, "sp", [(dev, dev ^ hop) for dev in range(4)]
+        )
     return (target_grad, source_grad, out_weight_grad)
 
 

time: 358 us -> 373 us (1.042)
  other arithmetic: 12.3 us -> 19.8 us
  waiting for transfers between devices: 130 us -> 134 us
    psum x1 -> x0, waiting for transfers between devices: 86.2 us -> none  [body(): out_weight_grad = lax.psum(weight_part, 'sp')]
    ppermute x0 -> x2, waiting for transfers between devices: none -> 84.4 us  [body(): lax.ppermute(out_weight_grad, 'sp', [(dev, dev ^ hop) for dev in range(4)])]
    unnamed x6 -> x5, waiting for transfers between devices: 25.1 us -> 34 us
    add x0 -> x2, other arithmetic: none -> 5.83 us  [body(): out_weight_grad + lax.ppermute(out_weight_grad, 'sp', [(dev, dev ^ hop) f...]
    unnamed x45 -> x56, local copies, waits for them, and re-layouts: 10.9 us -> 11.6 us
  transfers between devices with their start and end apart: 9 -> 10, of which waited for: 5 -> 4; matrix products, arithmetic and copies ran while one was open for 11% -> 14% of each run, Pallas kernels for 0% -> 0%
where the time goes in v1:
time: 373 us; the launch traced here: 371 us
  waiting for transfers between devices  134 us (36%)
  blocking collectives  114 us (31%)
  matrix products  49.6 us (13%)
  local copies, waits for them, and re-layouts  21.2 us (6%)
  other arithmetic  19.8 us (5%)
  starting transfers between devices  17.7 us (5%)
  between operations  14.3 us (4%)
    ppermute x2, waiting for transfers between devices, body(): lax.ppermute(out_weight_grad, 'sp', [(dev, dev ^ hop) for dev in range(4)])  84.4 us
    unnamed x5, waiting for transfers between devices  34 us
    all_gather x2, blocking collectives, body(): pieces = lax.all_gather((normed_t, out_cotangent), 'tp', axis=0, tiled=True)  23.7 us
    all_gather x1, blocking collectives, body(): lax.all_gather(key_flat, 'sp', axis=0, tiled=True)  16.3 us
    all_gather x1, blocking collectives, body(): lax.all_gather(value_flat, 'sp', axis=0, tiled=True)  16 us
    all_gather x1, blocking collectives, body(): lax.all_gather(d_attended, 'sp', axis=0, tiled=True)  15.1 us
    all_gather x1, blocking collectives, body(): lax.all_gather(queries, 'sp', axis=0, tiled=True)  15 us
    all_gather x1, blocking collectives, body(): lax.all_gather(log_total, 'sp', axis=0, tiled=True)  14.6 us
  transfers between devices with their start and end apart: 10, of which 4 were waited for; matrix products, arithmetic and copies ran while one was open for 14% of the time, Pallas kernels for 0%

profile of v1, /device:TPU:0, one launch (start us, length us, event | category | flops | bytes accessed | tf_op | source)
XLA Modules:
  0.0 371.3 jit_solution(3008800122920127305)
XLA Ops:
  11.3 11.9 %all_gather.31 = bf16[192,2048]{1,0:T(8,128)(2,1)S(1)} all-gather(bf16[24,2048]{1,0:T(8,128)(2,1)S(1)} %fusion.44), channel_id=1, replica_groups=mesh['sp'=4,'tp'=8] {'tp'}, dimensions={0}, use_global_device_ids=true | all-gather | bytes 884736 | tf_op jit(solution)/shard_map/all_gather | solution.py:71
  24.4 15.0 %all_gather.32 = bf16[768,256]{1,0:T(8,128)(2,1)S(1)} all-gather(bf16[192,256]{1,0:T(8,128)(2,1)S(1)} %convolution_convert_fusion.3), channel_id=1, replica_groups=mesh['sp'=4,'tp'=8] {'sp'}, dimensions={0}, use_global_device_ids=true | all-gather | bytes 491520 | tf_op jit(solution)/shard_map/all_gather | solution.py:132
  40.8 11.8 %all_gather.37 = bf16[192,2048]{1,0:T(8,128)(2,1)S(1)} all-gather(bf16[24,2048]{1,0:T(8,128)(2,1)} %param.19), channel_id=1, replica_groups=mesh['sp'=4,'tp'=8] {'tp'}, dimensions={0}, use_global_device_ids=true | all-gather | bytes 884736 | tf_op jit(solution)/shard_map/all_gather | solution.py:71
  56.1 3.4 all-to-all-start
  59.5 11.9 %all-gather.7.cloned.1.call-done = bf16[2048,512]{1,0:T(8,128)(2,1)} async-done(((bf16[256,512]{1,0:T(8,128)(2,1)}), bf16[2048,512]{1,0:T(8,128)(2,1)}) %all-gather.7.cloned.1.call-update) | async-done | bytes 2097168 | tf_op jit(solution)/shard_map/all_gather | solution.py:52
  74.2 3.4 all-to-all-start.1
  78.4 16.3 %all_gather.33 = bf16[4096,64]{0,1:T(8,128)(2,1)S(1)} all-gather(bf16[1024,64]{0,1:T(8,128)(2,1)S(1)} %bitcast.239), channel_id=1, replica_groups=mesh['sp'=4,'tp'=8] {'sp'}, dimensions={0}, use_global_device_ids=true | all-gather | bytes 655360 | tf_op jit(solution)/shard_map/all_gather | solution.py:88
  95.5 16.0 %all_gather.35 = bf16[4096,64]{0,1:T(8,128)(2,1)S(1)} all-gather(bf16[1024,64]{0,1:T(8,128)(2,1)S(1)} %bitcast.240), channel_id=1, replica_groups=mesh['sp'=4,'tp'=8] {'sp'}, dimensions={0}, use_global_device_ids=true | all-gather | bytes 655360 | tf_op jit(solution)/shard_map/all_gather | solution.py:89
  111.5 23.2 %while.3 = (s32[]{:T(128)}, f32[1,4,192]{2,1,0:T(4,128)S(1)}, f32[1,4,192]{2,1,0:T(4,128)S(1)}, f32[1,4,192,64]{2,3,1,0:T(8,128)S(1)}, s32[2]{0:T(128)S(1)}, /*i...) while((s32[]{:T(128)}, f32[1,4,192]{2,1,0:T(4,128)S(1)}, ...), condition=%wide.region_5.6_spmd.clone, body=%wide.region_2.5_spmd.clone.sunk | while | flops 415388160 | bytes 45173076 | solution.py:116
  112.7 4.6 %bitcast_reduce_fusion.3 = (f32[4,192]{1,0:T(4,128)S(1)}, f32[2048,192,4]{0,1,2:T(8,128)}) fusion(bf16[192,1,4,64]{0,3,2,1:T(8,128)(2,1)} %get-tuple-element.230, bf16[4096,64]{0,1:T(8,128)(2,1)S(1)} %get-tuple-element.229, s32[]{:T(128)S(6)} %select_n.6), kind=kOutput, calls=%fused_computation.1.clone.1 | convolution fusion | flops 204471552 | bytes 6654980 | tf_op jit(solution)/shard_map/while/body/eval_jaxpr/tgqd,sgd->gqts/dot_general | solution.py:101
  117.3 4.3 %fusion.90 = f32[1,4,192,64]{2,3,1,0:T(8,128)S(1)} fusion(f32[2048,192,4]{0,1,2:T(8,128)} %get-tuple-element.198, f32[4,192]{1,0:T(4,128)S(1)} %bitcast.230, f32[1,4,192,64]{2,3,1,0:T(8,128)S(1)} %get-tuple-element.215, bf16[4096,64]{0,1:T(8,128)(2,1)S(1)} %get-tuple-element.231, s32[]{:T(128)S(6)} %select_n.6, f32[4,192]{1,0:T(4,128)S(1)} %get-tuple-element.199, ...), kind=kOutput, calls=%fused_computation.8.clone.1 | convolution fusion | flops 206192640 | bytes 7020549 | tf_op jit(solution)/shard_map/while/body/eval_jaxpr/gqts,sgd->gqtd/dot_general | solution.py:108
  124.3 4.6 %bitcast_reduce_fusion.3 = (f32[4,192]{1,0:T(4,128)S(1)}, f32[2048,192,4]{0,1,2:T(8,128)}) fusion(bf16[192,1,4,64]{0,3,2,1:T(8,128)(2,1)} %get-tuple-element.230, bf16[4096,64]{0,1:T(8,128)(2,1)S(1)} %get-tuple-element.229, s32[]{:T(128)S(6)} %select_n.6), kind=kOutput, calls=%fused_computation.1.clone.1 | convolution fusion | flops 204471552 | bytes 6654980 | tf_op jit(solution)/shard_map/while/body/eval_jaxpr/tgqd,sgd->gqts/dot_general | solution.py:101
  128.9 4.3 %fusion.90 = f32[1,4,192,64]{2,3,1,0:T(8,128)S(1)} fusion(f32[2048,192,4]{0,1,2:T(8,128)} %get-tuple-element.198, f32[4,192]{1,0:T(4,128)S(1)} %bitcast.230, f32[1,4,192,64]{2,3,1,0:T(8,128)S(1)} %get-tuple-element.215, bf16[4096,64]{0,1:T(8,128)(2,1)S(1)} %get-tuple-element.231, s32[]{:T(128)S(6)} %select_n.6, f32[4,192]{1,0:T(4,128)S(1)} %get-tuple-element.199, ...), kind=kOutput, calls=%fused_computation.8.clone.1 | convolution fusion | flops 206192640 | bytes 7020549 | tf_op jit(solution)/shard_map/while/body/eval_jaxpr/gqts,sgd->gqtd/dot_general | solution.py:108
  136.6 15.1 %all_gather.38 = bf16[768,256]{1,0:T(8,128)(2,1)S(1)} all-gather(bf16[192,256]{1,0:T(8,128)(2,1)S(1)} %get-tuple-element.140), channel_id=1, replica_groups=mesh['sp'=4,'tp'=8] {'sp'}, dimensions={0}, use_global_device_ids=true | all-gather | bytes 491520 | tf_op jit(solution)/shard_map/all_gather | solution.py:133
  152.1 13.2 %all-gather.1 = f32[4,192,4]{1,2,0:T(4,128)S(1)} all-gather(f32[1,192,4]{1,2,0:T(4,128)S(1)} %bitcast.250), channel_id=1, replica_groups=mesh['sp'=4,'tp'=8] {'sp'}, dimensions={0}, use_global_device_ids=true | all-gather | bytes 15360 | tf_op jit(solution)/shard_map/all_gather | solution.py:137
  165.6 14.6 %all-gather = f32[768,1,4]{2,1,0:T(1,128)S(1)} all-gather(f32[192,1,4]{2,1,0:T(1,128)S(1)} %bitcast.247), channel_id=2, replica_groups=mesh['sp'=4,'tp'=8] {'sp'}, dimensions={0}, use_global_device_ids=true | all-gather | bytes 15360 | tf_op jit(solution)/shard_map/all_gather | solution.py:136
  183.1 3.2 fusion.27
  194.5 32.6 %reduce-scatter.7.cloned.1.call-done = f32[192,256]{1,0:T(8,128)} async-done(((f32[768,256]{1,0:T(8,128)}), f32[192,256]{1,0:T(8,128)}) %reduce-scatter.7.cloned.1.call-update) | async-done | bytes 196624
  231.4 5.4 %fusion.35 = bf16[1024,1,64]{0,2,1:T(8,128)(2,1)} fusion(bf16[768,4,64]{0,2,1:T(8,128)(2,1)S(1)} %bitcast.225, bf16[4,768,1024]{1,2,0:T(8,128)(2,1)} %copy-done.3), kind=kOutput, calls=%fused_computation.43 | convolution fusion | flops 402784256 | bytes 6815744 | tf_op jit(solution)/shard_map/while/body/eval_jaxpr/gqts,tgqd->sgd/dot_general | solution.py:173
  240.0 3.7 all-to-all-start.2
  243.7 7.0 %fusion.31 = bf16[1024,1,64]{0,2,1:T(8,128)(2,1)S(1)} fusion(bf16[768,4,64]{0,2,1:T(8,128)(2,1)} %bitcast.228, f32[1024,768,4]{1,0,2:T(8,128)} %copy-done.2, f32[4,768]{1,0:T(4,128)S(1)} %copy.81), kind=kOutput, calls=%fused_computation.40 | convolution fusion | flops 412090368 | bytes 13119488 | tf_op jit(solution)/shard_map/while/body/eval_jaxpr/gqts,tgqd->sgd/dot_general | solution.py:155
  253.9 4.2 %all-to-all-start.3 = ((bf16[8,2,4096]{2,1,0:T(2,128)(2,1)}), bf16[8,2,4096]{2,1,0:T(2,128)(2,1)}, u32[]{:S(2)}, u32[]{:S(2)}) async-start(bf16[8,2,4096]{2,1,0:T(2,128)(2,1)} %reshape.189), calls=%async_computation.4 | async-start | bytes 262144 | tf_op jit(solution)/shard_map/all_to_all | solution.py:190
  260.4 3.3 all-to-all-done.3
  277.2 84.4 %collective-permute-done.1 = f32[256,2048]{1,0:T(8,128)} collective-permute-done((f32[256,2048]{1,0:T(8,128)S(1)}, f32[256,2048]{1,0:T(8,128)}, u32[]{:S(2)}, u32[]{:S(2)}) %collective-permute-start.1) | collective-permute-done | bytes 2097184 | tf_op jit(solution)/shard_map/ppermute | solution.py:215
  (145 shorter events, 61.7 us)
Async XLA Ops:
  7.2 16.1 %copy-start = (bf16[2048,256]{1,0:T(8,128)(2,1)S(1)}, bf16[2048,256]{1,0:T(8,128)(2,1)}, u32[]{:S(2)}) copy-start(bf16[2048,256]{1,0:T(8,128)(2,1)} %param.15) | copy-start | bytes 3145732
  7.2 46.0 %copy-start.6 = (bf16[128,2048]{1,0:T(8,128)(2,1)S(1)}, bf16[128,2048]{1,0:T(8,128)(2,1)}, u32[]{:S(2)}) copy-start(bf16[128,2048]{1,0:T(8,128)(2,1)} %param.12) | copy-start | bytes 1572868
  7.2 46.0 %copy-start.17 = (f32[2048]{0:T(1024)S(1)}, f32[2048]{0:T(1024)}, u32[]{:S(2)}) copy-start(f32[2048]{0:T(1024)} %param.14) | copy-start | bytes 24580
  7.2 46.0 %all-gather.5.cloned.1.call-start = ((), (), s32[]{:S(2)}) async-start(), calls=%async_computation.6 | async-start | bytes 2359296 | tf_op jit(solution)/shard_map/all_gather | solution.py:51
  7.9 63.4 %all-gather.7.cloned.1.call-start = ((), (), s32[]{:S(2)}) async-start(), calls=%async_computation.7 | async-start | bytes 2359296 | tf_op jit(solution)/shard_map/all_gather | solution.py:52
  52.6 82.3 %copy-start.5 = (bf16[192,2048]{1,0:T(8,128)(2,1)}, bf16[192,2048]{1,0:T(8,128)(2,1)S(1)}, u32[]{:S(2)}) copy-start(bf16[192,2048]{1,0:T(8,128)(2,1)S(1)} %all_gather.37) | copy-start | bytes 2359300
  53.2 42.3 %copy-start.21 = (f32[128]{0:T(128)}, f32[128]{0:T(128)S(1)}, u32[]{:S(2)}) copy-start(f32[128]{0:T(128)S(1)} %get-tuple-element.136) | copy-start | bytes 1540
  56.1 18.1 %all-to-all-start = ((bf16[128,8,64]{0,2,1:T(8,128)(2,1)}), bf16[128,8,64]{0,2,1:T(8,128)(2,1)S(1)}, u32[]{:S(2)}, u32[]{:S(2)}) async-start(bf16[128,8,64]{0,2,1:T(8,128)(2,1)} %bitcast), calls=%async_computation | async-start | bytes 262144 | tf_op jit(solution)/shard_map/all_to_all | solution.py:65
  74.2 20.5 %all-to-all-start.1 = ((bf16[128,8,64]{0,2,1:T(8,128)(2,1)}), bf16[128,8,64]{0,2,1:T(8,128)(2,1)S(1)}, u32[]{:S(2)}, u32[]{:S(2)}) async-start(bf16[128,8,64]{0,2,1:T(8,128)(2,1)} %bitcast.7), calls=%async_computation.1 | async-start | bytes 262144 | tf_op jit(solution)/shard_map/all_to_all | solution.py:66
  77.6 149.5 %reduce-scatter.7.cloned.1.call-start = ((), (), s32[]{:S(2)}) async-start(), calls=%async_computation.9 | async-start | bytes 983040
  117.3 5.8 %copy-start.24 = (s32[2]{0:T(128)S(1)}, s32[2]{0:T(128)}, u32[]{:S(2)}) copy-start(s32[2]{0:T(128)} %copy-done.23) | copy-start | bytes 28 | tf_op jit(solution)/shard_map/while
  134.8 48.3 %copy-start.13 = (bf16[1,4,192,64]{2,3,1,0:T(8,128)(2,1)}, bf16[1,4,192,64]{2,3,1,0:T(8,128)(2,1)S(1)}, u32[]{:S(2)}) copy-start(bf16[1,4,192,64]{2,3,1,0:T(8,128)(2,1)S(1)} %divide_convert_fusion) | copy-start | bytes 294916
  151.9 31.2 %copy-start.8 = (bf16[768,256]{0,1:T(8,128)(2,1)}, bf16[768,256]{0,1:T(8,128)(2,1)S(1)}, u32[]{:S(2)}) copy-start(bf16[768,256]{0,1:T(8,128)(2,1)S(1)} %copy.82) | copy-start | bytes 1179652
  191.4 83.0 %reduce-scatter.5.cloned.1.call-start = ((), (), s32[]{:S(2)}) async-start(), calls=%async_computation.8 | async-start | bytes 1769472 | tf_op jit(solution)/shard_map/reduce_scatter | solution.py:203
  193.1 46.9 %copy-start.4 = (f32[256,2048]{1,0:T(8,128)}, f32[256,2048]{1,0:T(8,128)S(1)}, u32[]{:S(2)}) copy-start(f32[256,2048]{1,0:T(8,128)S(1)} %fusion.56) | copy-start | bytes 6291460
  193.1 73.8 %collective-permute-start = (f32[256,2048]{1,0:T(8,128)S(1)}, f32[256,2048]{1,0:T(8,128)}, u32[]{:S(2)}, u32[]{:S(2)}) collective-permute-start(f32[256,2048]{1,0:T(8,128)S(1)} %fusion.56), channel_id=1, source_target_pairs={{0,8},{8,0},{16,24},{24,16},{1,9},{9,1},{17,25},{25,17},{2,10},{10... | collective-permute-start | bytes 6291464 | tf_op jit(solution)/shard_map/ppermute | solution.py:215
  240.0 13.9 %all-to-all-start.2 = ((bf16[8,2,4096]{2,1,0:T(2,128)(2,1)}), bf16[8,2,4096]{2,1,0:T(2,128)(2,1)S(1)}, u32[]{:S(2)}, u32[]{:S(2)}) async-start(bf16[8,2,4096]{2,1,0:T(2,128)(2,1)} %reshape.187), calls=%async_computation.3 | async-start | bytes 262144 | tf_op jit(solution)/shard_map/all_to_all | solution.py:189
  253.9 9.8 %all-to-all-start.3 = ((bf16[8,2,4096]{2,1,0:T(2,128)(2,1)}), bf16[8,2,4096]{2,1,0:T(2,128)(2,1)}, u32[]{:S(2)}, u32[]{:S(2)}) async-start(bf16[8,2,4096]{2,1,0:T(2,128)(2,1)} %reshape.189), calls=%async_computation.4 | async-start | bytes 262144 | tf_op jit(solution)/shard_map/all_to_all | solution.py:190
  259.2 12.9 %copy-start.18 = (f32[2048]{0:T(1024)S(1)}, f32[2048]{0:T(1024)}, u32[]{:S(2)}) copy-start(f32[2048]{0:T(1024)} %param.14) | copy-start | bytes 24580
  266.9 6.1 %copy-start.20 = (f32[128]{0:T(128)S(1)}, f32[128]{0:T(128)}, u32[]{:S(2)}) copy-start(f32[128]{0:T(128)} %get-tuple-element.135) | copy-start | bytes 1540
  266.9 6.1 %copy-start.22 = (f32[128]{0:T(128)S(1)}, f32[128]{0:T(128)}, u32[]{:S(2)}) copy-start(f32[128]{0:T(128)} %copy-done.21) | copy-start | bytes 1540
  269.6 5.8 %copy-start.15 = (bf16[24,2048]{1,0:T(8,128)(2,1)S(1)}, bf16[24,2048]{1,0:T(8,128)(2,1)}, u32[]{:S(2)}) copy-start(bf16[24,2048]{1,0:T(8,128)(2,1)} %param.19) | copy-start | bytes 294916
  269.6 5.8 %copy-start.19 = (f32[24]{0:T(128)S(1)}, f32[24]{0:T(128)}, u32[]{:S(2)}) copy-start(f32[24]{0:T(128)} %get-tuple-element.137) | copy-start | bytes 292
  269.7 92.0 %collective-permute-start.1 = (f32[256,2048]{1,0:T(8,128)S(1)}, f32[256,2048]{1,0:T(8,128)}, u32[]{:S(2)}, u32[]{:S(2)}) collective-permute-start(f32[256,2048]{1,0:T(8,128)S(1)} %add.67), channel_id=1, source_target_pairs={{0,16},{8,24},{16,0},{24,8},{1,17},{9,25},{17,1},{25,9},{2,18},{10... | collective-permute-start | bytes 6291464 | tf_op jit(solution)/shard_map/ppermute | solution.py:215
  (14 other events, 56.2 us)
Sparse Core Ops, SparseCore 0:
  9.9 30.4 all-gather.4
  42.3 28.9 all-gather.6
  191.5 35.5 reduce-scatter.6
  231.6 37.4 reduce-scatter.4
